TPU v7x, 32 devices: a whole 2x2x4 slice. The times are simulated.
32 devices in a mesh: ep: 8 (over z, core), tp: 4 (over y, x).
Axes of the slice: x: 2, y: 2, z: 4, core: 2. Of those that a mesh axis runs over, the one named last changes fastest.
Arguments:
- tokens: bfloat16 [2048, 2048], P('ep', 'tp'), may hold values from -800 to 800
- norm_gain: bfloat16 [2048], P('tp'), may hold values from 0.099609375 to 1.8984375
- w_gate: bfloat16 [8, 2048, 6144], P('ep', None, 'tp'), may hold values from -0.125 to 0.125
- w_up: bfloat16 [8, 2048, 6144], P('ep', None, 'tp'), may hold values from -0.125 to 0.125
- w_down: bfloat16 [8, 6144, 2048], P('ep', 'tp'), may hold values from -1.2757759 to 1.2757759
- routes: int32 [2048, 2], P('ep'), may hold values from 0 to 7, all different within a row; in each aligned block of 256 rows (0 to 255, 256 to 511, ...) at most 128 rows name the same one
- route_weights: float32 [2048, 2], P('ep'), may hold values from 0.1 to 1
- final_gain: bfloat16 [2048], P('tp'), may hold values from 0.099609375 to 1.8984375
Outputs:
- mixed_out: bfloat16 [2048, 2048], P('ep', 'tp')
Inputs may be any that keep to these rules, and one draw needn't show every extreme that they name: `routes`: A token's 2 experts differ. Among the tokens of one index of ep (aligned blocks of 256 rows), no expert is named by more than 128 tokens, a bound that some block reaches.
All inputs are finite; a program needn't handle non-finite values.
Results may differ from a plain program's by a relative error of at most 0.017.
Values may be sent and summed in bfloat16 or wider, within the bound.
A program may use at most 64 MiB of HBM per device.

v0:
```python
import jax
import jax.numpy as jnp
from jax import lax
from jax.sharding import PartitionSpec as P

EPS = 1e-06


def slot_targets(routes, experts, capacity):
    flat = routes.reshape(-1)
    onehot = (flat[:, None] == jnp.arange(experts, dtype=jnp.int32)[None, :]).astype(jnp.int32)
    before = jnp.cumsum(onehot, axis=0) - onehot
    slot = jnp.sum(before * onehot, axis=1)
    return flat * capacity + slot


def local(tokens, norm_gain, w_gate, w_up, w_down, routes, route_weights, final_gain):
    experts = lax.axis_size("ep")
    tok_rows = tokens.shape[0]
    share = tokens.shape[1]
    width = share * lax.axis_size("tp")
    topk = routes.shape[1]
    capacity = 2 * tok_rows * topk // experts
    wide = tokens.astype(jnp.float32)
    input_squares = lax.psum(jnp.sum(wide * wide, axis=1), "tp")
    scale = lax.rsqrt(input_squares / width + EPS)
    normed = (wide * scale[:, None] * norm_gain.astype(jnp.float32)[None, :]).astype(jnp.bfloat16)
    target = slot_targets(routes, experts, capacity)
    sources = jnp.repeat(jnp.arange(tok_rows, dtype=jnp.int32), topk)
    gate_w = w_gate[0]
    up_w = w_up[0]
    down_w = w_down[0]
    outbox = jnp.zeros((experts * capacity, share), jnp.bfloat16).at[target].set(normed[sources])
    inbox = lax.all_to_all(outbox, "ep", split_axis=0, concat_axis=0, tiled=True)
    piece = lax.all_gather(inbox, "tp", axis=1, tiled=True)
    gate = jnp.dot(piece, gate_w, preferred_element_type=jnp.float32)
    up = jnp.dot(piece, up_w, preferred_element_type=jnp.float32)
    hidden = (jax.nn.silu(gate) * up).astype(jnp.bfloat16)
    sums = lax.psum_scatter(
        lax.dot_general(
            down_w, hidden, (((0,), (1,)), ((), ())), preferred_element_type=jnp.float32
        ).astype(jnp.bfloat16),
        "tp",
        scatter_dimension=0,
        tiled=True,
    )
    returned = lax.all_to_all(sums, "ep", split_axis=1, concat_axis=1, tiled=True)
    picked = jnp.take(returned, target, axis=1).reshape(returned.shape[0], tok_rows, topk)
    combined = jnp.einsum("dtk,tk->td", picked.astype(jnp.float32), route_weights)
    local_squares = jnp.sum(combined * combined, axis=1)
    total_squares = lax.psum(local_squares, "tp")
    final_scale = lax.rsqrt(total_squares / width + EPS)
    return (combined * final_scale[:, None] * final_gain.astype(jnp.float32)[None, :]).astype(
        jnp.bfloat16
    )


def solution(mesh):
    in_specs = (
        P("ep", "tp"),
        P("tp"),
        P("ep", None, "tp"),
        P("ep", None, "tp"),
        P("ep", "tp", None),
        P("ep", None),
        P("ep", None),
        P("tp"),
    )
    out_specs = P("ep", "tp")
    return jax.shard_map(local, mesh=mesh, in_specs=in_specs, out_specs=out_specs, check_vma=False)
```

profile of v0, /device:TPU:0, one launch (start us, length us, event | category | flops | bytes accessed | tf_op | source)
XLA Modules:
  0.0 247.3 jit_solution(9177944375881044333)
XLA Ops:
  6.5 0.8 copy.13
  7.4 0.1 eq.26
  7.5 0.1 reshape.101
  7.6 0.7 broadcast_multiply_fusion
  8.3 1.1 reduce-window.6
  9.5 0.2 slice_reduce_fusion
  9.7 0.1 copy.17
  9.9 0.1 mul.70
  10.0 1.1 fusion.12
  11.1 11.4 %psum.14 = f32[256]{0:T(256)S(1)} all-reduce(f32[256]{0:T(256)S(1)} %fusion.12), channel_id=1, replica_groups=mesh['ep'=8,'tp'=4] {'tp'}, use_global_device_ids=true, to_apply=%region_4.5 | all-reduce | flops 256 | bytes 2048 | tf_op jit(solution)/shard_map/psum | solution.py:25
  22.5 0.7 convert_element_type.35
  23.2 0.1 reshape.103
  23.4 0.1 fusion.24
  23.5 1.1 fusion.14
  24.5 5.0 %scatter_custom_fusion = bf16[1024,512]{1,0:T(8,128)(2,1)S(1)} fusion(s32[512]{0:T(512)S(1)} %bitcast.54, bf16[256,512]{1,0:T(8,128)(2,1)S(1)} %fusion.14, s32[1024]{0:T(1024)S(1)} %pad_clamp_fusion.1, bf16[]{:T(256)} %constant.18.clone.1), kind=kCustom, calls=%fused_computation.22 | custom fusion | bytes 1048578 | tf_op jit(solution)/shard_map/scatter | solution.py:33
  29.6 31.3 %all_to_all.24 = bf16[8,128,512]{2,1,0:T(8,128)(2,1)} all-to-all(bf16[8,128,512]{2,1,0:T(8,128)(2,1)S(1)} %bitcast.50), channel_id=1, replica_groups=mesh['ep'=8,'tp'=4] {'ep'}, dimensions={0} | all-to-all | bytes 2097152 | tf_op jit(solution)/shard_map/all_to_all | solution.py:34
  61.0 0.2 reduce-scatter.2.cloned.1.call-start
  61.2 49.4 %all-gather.2.cloned.1.call-done = bf16[1024,2048]{1,0:T(8,128)(2,1)} async-done(((bf16[1024,512]{1,0:T(8,128)(2,1)}), bf16[1024,2048]{1,0:T(8,128)(2,1)}) %all-gather.2.cloned.1.call-update) | async-done | bytes 4194320 | tf_op jit(solution)/shard_map/all_gather | solution.py:35
  110.6 11.7 %fusion.4 = f32[1024,1536]{1,0:T(8,128)} fusion(bf16[1024,2048]{1,0:T(8,128)(2,1)} %all-gather.2.cloned.1.call-done, bf16[1,2048,1536]{2,1,0:T(8,128)(2,1)} %param.10), kind=kOutput, calls=%fused_computation.7 | convolution fusion | flops 6442450944 | bytes 16777216 | tf_op jit(solution)/shard_map/dot_general | solution.py:36
  122.3 21.0 %convert_bitcast_fusion = bf16[2048,1024]{0,1:T(8,128)(2,1)} fusion(bf16[1,1536,2048]{2,1,0:T(8,128)(2,1)} %param.12, f32[1024,1536]{1,0:T(8,128)} %fusion.4, bf16[1024,2048]{1,0:T(8,128)(2,1)} %all-gather.2.cloned.1.call-done, bf16[1,2048,1536]{2,1,0:T(8,128)(2,1)} %param.11), kind=kOutput, calls=%fused_computation.10 | convolution fusion | flops 12896436224 | bytes 27262976 | tf_op jit(solution)/shard_map/dot_general | solution.py:40
  143.4 52.7 %reduce-scatter.2.cloned.1.call-done = bf16[512,1024]{0,1:T(8,128)(2,1)} async-done(((bf16[2048,1024]{0,1:T(8,128)(2,1)}), bf16[512,1024]{0,1:T(8,128)(2,1)}) %reduce-scatter.2.cloned.1.call-update) | async-done | bytes 1048592 | tf_op jit(solution)/shard_map/reduce_scatter | solution.py:39
  196.1 4.6 %all-to-all-start.1 = ((bf16[512,8,128]{0,2,1:T(8,128)(2,1)}), bf16[512,8,128]{0,2,1:T(8,128)(2,1)S(1)}, u32[]{:S(2)}, u32[]{:S(2)}) async-start(bf16[512,8,128]{0,2,1:T(8,128)(2,1)} %bitcast.52), calls=%async_computation.2 | async-start | bytes 2097152 | tf_op jit(solution)/shard_map/all_to_all | solution.py:47
  200.7 0.1 reduce_sum.32
  201.0 0.2 copy.16
  201.1 0.2 copy.18
  201.4 25.9 %all-to-all-done.1 = bf16[512,8,128]{0,2,1:T(8,128)(2,1)S(1)} async-done(((bf16[512,8,128]{0,2,1:T(8,128)(2,1)}), bf16[512,8,128]{0,2,1:T(8,128)(2,1)S(1)}, u32[]{:S(2)}, u32[]{:S(2)}) %all-to-all-start.1) | async-done | bytes 1048608 | tf_op jit(solution)/shard_map/all_to_all | solution.py:47
  227.3 2.0 gather_fusion
  229.2 0.2 gather.11
  229.5 1.1 fusion.21
  230.5 0.1 fusion.15
  230.6 9.0 %psum.15 = f32[256]{0:T(256)S(1)} all-reduce(f32[256]{0:T(256)S(1)} %fusion.15), channel_id=1, replica_groups=mesh['ep'=8,'tp'=4] {'tp'}, use_global_device_ids=true, to_apply=%region_8.9 | all-reduce | flops 256 | bytes 2048 | tf_op jit(solution)/shard_map/psum | solution.py:51
  239.6 0.8 fusion.17
  (22 shorter events, 0.2 us)
Async XLA Ops:
  6.5 104.1 %all-gather.2.cloned.1.call-start = ((), (), s32[]{:S(2)}) async-start(), calls=%async_computation.3 | async-start | bytes 5242880 | tf_op jit(solution)/shard_map/all_gather | solution.py:35
  61.0 135.1 %reduce-scatter.2.cloned.1.call-start = ((), (), s32[]{:S(2)}) async-start(), calls=%async_computation.4 | async-start | bytes 5242880 | tf_op jit(solution)/shard_map/reduce_scatter | solution.py:39
  143.3 57.6 %copy-start = (s32[256,2]{0,1:T(2,128)S(1)}, s32[256,2]{0,1:T(2,128)}, u32[]{:S(2)}) copy-start(s32[256,2]{0,1:T(2,128)} %param.13) | copy-start | bytes 6148
  143.3 57.8 %copy-start.1 = (f32[256,2]{0,1:T(2,128)S(1)}, f32[256,2]{0,1:T(2,128)}, u32[]{:S(2)}) copy-start(f32[256,2]{0,1:T(2,128)} %param.14) | copy-start | bytes 6148
  143.3 58.0 %copy-start.2 = (bf16[512]{0:T(512)(128)(2,1)S(1)}, bf16[512]{0:T(512)(128)(2,1)}, u32[]{:S(2)}) copy-start(bf16[512]{0:T(512)(128)(2,1)} %param.15) | copy-start | bytes 3076
  196.1 31.2 %all-to-all-start.1 = ((bf16[512,8,128]{0,2,1:T(8,128)(2,1)}), bf16[512,8,128]{0,2,1:T(8,128)(2,1)S(1)}, u32[]{:S(2)}, u32[]{:S(2)}) async-start(bf16[512,8,128]{0,2,1:T(8,128)(2,1)} %bitcast.52), calls=%async_computation.2 | async-start | bytes 2097152 | tf_op jit(solution)/shard_map/all_to_all | solution.py:47
Sparse Core Ops, SparseCore 0:
  61.1 49.4 all-gather.1
  143.5 52.5 reduce-scatter.1
where the time goes:
time: 248 us; the launch traced here: 247 us
  waiting for transfers between devices  128 us (52%)
  blocking collectives  51.7 us (21%)
  matrix products  33.8 us (14%)
  between operations  13.6 us (5%)
  local copies, waits for them, and re-layouts  9.53 us (4%)
  other arithmetic  5.79 us (2%)
  starting transfers between devices  4.83 us (2%)
    reduce_scatter x1, waiting for transfers between devices, local(): lax.psum_scatter(lax.dot_general(down_w, hidden, (((0,), (1,)), ((), ()))...  52.7 us
    all_gather x1, waiting for transfers between devices, local(): piece = lax.all_gather(inbox, 'tp', axis=1, tiled=True)  49.4 us
    all_to_all x1, blocking collectives, local(): lax.all_to_all(outbox, 'ep', split_axis=0, concat_axis=0, tiled=True)  31.3 us
    all_to_all x1, waiting for transfers between devices, local(): lax.all_to_all(sums, 'ep', split_axis=1, concat_axis=1, tiled=True)  25.9 us
    dot_general x1, matrix products, local(): lax.dot_general(down_w, hidden, (((0,), (1,)), ((), ())), preferred_eleme...  21 us
    dot_general x1, matrix products, local(): gate = jnp.dot(piece, gate_w, preferred_element_type=jnp.float32)  11.7 us
    psum x1, blocking collectives, local(): input_squares = lax.psum(jnp.sum(wide * wide, axis=1), 'tp')  11.4 us
    psum x1, blocking collectives, local(): total_squares = lax.psum(local_squares, 'tp')  8.95 us
  transfers between devices with their start and end apart: 3, of which 3 were waited for; matrix products, arithmetic and copies ran while one was open for 0% of the time, Pallas kernels for 0%

commit v1 on v0

--- a/solution.py
+++ b/solution.py
@@ -1,9 +1,15 @@
+import functools
+
 import jax
 import jax.numpy as jnp
 from jax import lax
+from jax.experimental import pallas as pl
+from jax.experimental.pallas import tpu as pltpu
 from jax.sharding import PartitionSpec as P
 
 EPS = 1e-06
+VMEM_LIMIT = 60 * 1024 * 1024
+F32, BF16 = jnp.float32, jnp.bfloat16
 
 
 def slot_targets(routes, experts, capacity):
@@ -55,6 +61,314 @@
     )
 
 
+def remote(src, dst, send, recv, device):
+    return pltpu.make_async_remote_copy(
+        src_ref=src, dst_ref=dst, send_sem=send, recv_sem=recv,
+        device_id=device, device_id_type=pl.DeviceIdType.MESH,
+    )
+
+
+def kernel(
+    n_ep, tokens, gain, wg_hbm, wu_hbm, wd_hbm, routes, weights, final_gain, out,
+    wg, wu, wd, pick, outbox, xbuf, gbuf, normed, hidden, pbuf, r1, s1, r2, fin, ret, stat,
+    w_sem, z_send, z_recv, ag_send, ag_recv, g_send, g_recv, r1_send, r1_recv,
+    r2_send, r2_recv, ret_send, ret_recv, st_send, st_recv,
+):
+    rows, share = tokens.shape
+    topk = routes.shape[1]
+    cap = outbox.shape[1]
+    width = 4 * share
+    pairs = n_ep // 2
+    me, q = lax.axis_index("ep"), lax.axis_index("tp")
+    nx, ny, nd = q + 1 - 2 * (q % 2), q + 2 - 4 * (q // 2), 3 - q
+    tp_peers = (nx, ny, nd)
+
+    def flip(k):
+        total, bit = 0, 1
+        while bit < n_ep:
+            total = total + bit * ((me // bit + k // bit) % 2)
+            bit *= 2
+        return total
+
+    loads = [
+        pltpu.make_async_copy(src, dst, w_sem.at[i])
+        for i, (src, dst) in enumerate(((wg_hbm, wg), (wu_hbm, wu), (wd_hbm, wd)))
+    ]
+    for load in loads:
+        load.start()
+
+    barrier = pltpu.get_barrier_semaphore()
+    for k in range(1, n_ep):
+        pl.semaphore_signal(barrier, inc=1, device_id={"ep": flip(k)}, device_id_type=pl.DeviceIdType.MESH)
+    for peer in tp_peers:
+        pl.semaphore_signal(barrier, inc=1, device_id={"tp": peer}, device_id_type=pl.DeviceIdType.MESH)
+
+    lane = lax.broadcasted_iota(jnp.int32, (rows, 128), 1)
+    named = [routes[:, k : k + 1] for k in range(topk)]
+    hot = sum((lane == named[k]).astype(F32) for k in range(topk)).astype(BF16)
+    earlier = (
+        lax.broadcasted_iota(jnp.int32, (rows, rows), 1) < lax.broadcasted_iota(jnp.int32, (rows, rows), 0)
+    ).astype(F32).astype(BF16)
+    before = jnp.dot(earlier, hot, preferred_element_type=F32)
+    column = lax.broadcasted_iota(jnp.int32, (rows, n_ep * cap), 1)
+    for k in range(topk):
+        slot = jnp.sum(jnp.where(lane == named[k], before, 0.0), axis=1, keepdims=True)
+        target = named[k] * cap + slot.astype(jnp.int32)
+        pick[k] = (column == target).astype(F32).astype(BF16)
+    for e in range(n_ep):
+        both = sum(pick[k, :, e * cap : (e + 1) * cap].astype(F32) for k in range(topk)).astype(BF16)
+        outbox[e] = lax.dot_general(
+            both, tokens[...], (((0,), (0,)), ((), ())), preferred_element_type=F32
+        ).astype(BF16)
+    gbuf[q] = gain[...]
+    xbuf[me, q] = outbox[me]
+    pl.semaphore_wait(barrier, n_ep - 1 + 3)
+
+    def gain_copy(i):
+        return remote(gain, gbuf.at[q], g_send.at[i], g_recv.at[i], {"tp": tp_peers[i]})
+
+    def out_copy(k):
+        c = flip(k)
+        return remote(outbox.at[c], xbuf.at[me, q], z_send.at[k], z_recv.at[k], {"ep": c})
+
+    def spread(k, i, relay=None):
+        c = flip(k)
+        if i < 2:
+            piece, to = q, (nx, ny)[i]
+        else:
+            piece, to = (ny, nx) [relay], (nx, ny)[relay]
+        return remote(xbuf.at[c, piece], xbuf.at[c, piece], ag_send.at[k, i], ag_recv.at[k, i], {"tp": to})
+
+    def first_sum(k, i, p):
+        c = flip(k)
+        to = (nx, ny)[p]
+        return remote(
+            pbuf.at[c, (to, nd)[i]], r1.at[c, i], r1_send.at[k, i], r1_recv.at[k, i], {"tp": to}
+        )
+
+    def second_sum(k, p):
+        c = flip(k)
+        return remote(s1.at[c], r2.at[c], r2_send.at[k], r2_recv.at[k], {"tp": (ny, nx)[p]})
+
+    def back(k):
+        c = flip(k)
+        return remote(fin.at[c], ret.at[me], ret_send.at[k], ret_recv.at[k], {"ep": c})
+
+    def gather_first(s):
+        for p in range(2):
+            k = 2 * s + p
+            if p == 0:
+                @pl.when(s > 0)
+                def _():
+                    out_copy(k).wait_recv()
+            else:
+                out_copy(k).wait_recv()
+            spread(k, p).start()
+            spread(k, 1 - p).start()
+
+    def gather_second(s):
+        for p in range(2):
+            k = 2 * s + p
+            spread(k, p).wait_recv()
+            spread(k, 2, 1 - p).start()
+
+    def compute(s):
+        for p in range(2):
+            k = 2 * s + p
+            c = flip(k)
+            spread(k, 1 - p).wait_recv()
+            spread(k, 2, 1 - p).wait_recv()
+            squares = jnp.zeros((cap, 1), F32)
+            for j in range(4):
+                wide = xbuf[c, j].astype(F32)
+                squares = squares + jnp.sum(wide * wide, axis=1, keepdims=True)
+            scale = lax.rsqrt(squares / width + EPS)
+            for j in range(4):
+                normed[p * cap : (p + 1) * cap, j * share : (j + 1) * share] = (
+                    xbuf[c, j].astype(F32) * scale * gbuf[j, 0:1, :]
+                ).astype(BF16)
+
+        @pl.when(s == 0)
+        def _():
+            loads[0].wait()
+            loads[1].wait()
+
+        tile = 256
+
+        @pl.loop(0, wg.shape[1] // tile)
+        def _(t):
+            cols = pl.ds(pl.multiple_of(t * tile, tile), tile)
+            gate = jnp.dot(normed[...], wg[:, cols], preferred_element_type=F32)
+            up = jnp.dot(normed[...], wu[:, cols], preferred_element_type=F32)
+            hidden[:, cols] = (gate / (1.0 + jnp.exp(-gate)) * up).astype(BF16)
+
+        @pl.when(s == 0)
+        def _():
+            loads[2].wait()
+
+        @pl.loop(0, 4)
+        def _(j):
+            cols = pl.ds(pl.multiple_of(j * share, share), share)
+            part = jnp.dot(hidden[...], wd[:, cols], preferred_element_type=F32).astype(BF16)
+            for p in range(2):
+                pbuf[flip(2 * s + p), j] = part[p * cap : (p + 1) * cap]
+
+        for i in (1, 0):
+            for p in range(2):
+                first_sum(2 * s + p, i, p).start()
+
+    def reduce_first(s):
+        for p in range(2):
+            k = 2 * s + p
+            c = flip(k)
+            first_sum(k, 1, p).wait_recv()
+            s1[c] = (pbuf[c, (ny, nx)[p]].astype(F32) + r1[c, 1].astype(F32)).astype(BF16)
+            second_sum(k, p).start()
+
+    def reduce_second(s):
+        for p in range(2):
+            k = 2 * s + p
+            c = flip(k)
+            first_sum(k, 0, p).wait_recv()
+            second_sum(k, p).wait_recv()
+            total = (pbuf[c, q].astype(F32) + r1[c, 0].astype(F32) + r2[c].astype(F32)).astype(BF16)
+            if p == 0:
+                @pl.when(s == 0)
+                def _():
+                    ret[me] = total
+
+                @pl.when(s > 0)
+                def _():
+                    fin[c] = total
+                    back(k).start()
+            else:
+                fin[c] = total
+                back(k).start()
+
+    for k in range(1, n_ep):
+        out_copy(k).start()
+    for i in range(3):
+        gain_copy(i).start()
+    gather_first(0)
+    gather_first(1)
+    gather_second(0)
+    gather_first(2)
+    for i in range(3):
+        gain_copy(i).wait_recv()
+
+    @pl.loop(0, pairs + 2)
+    def _(s):
+        @pl.when(s < pairs)
+        def _():
+            compute(s)
+
+        @pl.when(s + 1 < pairs)
+        def _():
+            gather_second(s + 1)
+
+        @pl.when(s + 3 < pairs)
+        def _():
+            gather_first(s + 3)
+
+        @pl.when((s >= 1) & (s < pairs + 1))
+        def _():
+            reduce_first(s - 1)
+
+        @pl.when(s >= 2)
+        def _():
+            reduce_second(s - 2)
+
+    for k in range(1, n_ep):
+        back(k).wait_recv()
+    combined = jnp.zeros((rows, share), F32)
+    for k in range(topk):
+        rowsof = jnp.dot(
+            pick[k], ret[...].reshape(n_ep * cap, share), preferred_element_type=F32
+        )
+        combined = combined + rowsof * weights[:, k : k + 1]
+    squares = jnp.sum(combined * combined, axis=1, keepdims=True)
+    same = lax.broadcasted_iota(jnp.int32, (rows, rows), 0) == lax.broadcasted_iota(jnp.int32, (rows, rows), 1)
+    line = jnp.sum(jnp.where(same, squares, 0.0), axis=0, keepdims=True)
+    stat[0] = jnp.broadcast_to(line, (8, rows))
+
+    def stat_copy(i):
+        return remote(stat.at[0], stat.at[1 + i], st_send.at[i], st_recv.at[i], {"tp": tp_peers[i]})
+
+    for i in range(3):
+        stat_copy(i).start()
+    for i in range(3):
+        stat_copy(i).wait_recv()
+    total = stat[0, 0:1] + stat[1, 0:1] + stat[2, 0:1] + stat[3, 0:1]
+    scale = lax.rsqrt(jnp.sum(jnp.where(same, total, 0.0), axis=1, keepdims=True) / width + EPS)
+    out[...] = (combined * scale * final_gain[0:1, :]).astype(BF16)
+
+    for i in range(3):
+        gain_copy(i).wait_send()
+        stat_copy(i).wait_send()
+    out_copy(1).wait_send()
+    back(1).wait_send()
+
+    @pl.loop(2, n_ep)
+    def _(k):
+        out_copy(k).wait_send()
+        back(k).wait_send()
+
+    @pl.loop(0, pairs)
+    def _(s):
+        for p in range(2):
+            k = 2 * s + p
+            spread(k, 0).wait_send()
+            spread(k, 1).wait_send()
+            spread(k, 2, 1 - p).wait_send()
+            first_sum(k, 0, p).wait_send()
+            first_sum(k, 1, p).wait_send()
+            second_sum(k, p).wait_send()
+
+
+def fused(tokens, norm_gain, w_gate, w_up, w_down, routes, route_weights, final_gain):
+    n_ep = lax.axis_size("ep")
+    rows, share = tokens.shape
+    topk = routes.shape[1]
+    cap = 2 * rows * topk // n_ep
+    depth, units = w_gate.shape[1:]
+    dma = pltpu.SemaphoreType.DMA
+    vmem = pl.BlockSpec(memory_space=pltpu.VMEM)
+    hbm = pl.BlockSpec(memory_space=pl.ANY)
+    gain8 = jnp.broadcast_to(norm_gain.astype(F32)[None, :], (8, share))
+    last8 = jnp.broadcast_to(final_gain.astype(F32)[None, :], (8, share))
+    return pl.pallas_call(
+        functools.partial(kernel, n_ep),
+        out_shape=jax.ShapeDtypeStruct((rows, share), BF16),
+        in_specs=[vmem, vmem, hbm, hbm, hbm, vmem, vmem, vmem],
+        out_specs=vmem,
+        scratch_shapes=[
+            pltpu.VMEM((depth, units), BF16),
+            pltpu.VMEM((depth, units), BF16),
+            pltpu.VMEM((units, depth), BF16),
+            pltpu.VMEM((topk, rows, n_ep * cap), BF16),
+            pltpu.VMEM((n_ep, cap, share), BF16),
+            pltpu.VMEM((n_ep, 4, cap, share), BF16),
+            pltpu.VMEM((4, 8, share), F32),
+            pltpu.VMEM((2 * cap, depth), BF16),
+            pltpu.VMEM((2 * cap, units), BF16),
+            pltpu.VMEM((n_ep, 4, cap, share), BF16),
+            pltpu.VMEM((n_ep, 2, cap, share), BF16),
+            pltpu.VMEM((n_ep, cap, share), BF16),
+            pltpu.VMEM((n_ep, cap, share), BF16),
+            pltpu.VMEM((n_ep, cap, share), BF16),
+            pltpu.VMEM((n_ep, cap, share), BF16),
+            pltpu.VMEM((4, 8, rows), F32),
+            dma((3,)), dma((n_ep,)), dma((n_ep,)), dma((n_ep, 3)), dma((n_ep, 3)),
+            dma((3,)), dma((3,)), dma((n_ep, 2)), dma((n_ep, 2)),
+            dma((n_ep,)), dma((n_ep,)), dma((n_ep,)), dma((n_ep,)), dma((3,)), dma((3,)),
+        ],
+        compiler_params=pltpu.CompilerParams(
+            collective_id=0, has_side_effects=True, vmem_limit_bytes=VMEM_LIMIT
+        ),
+        name="routed_experts",
+    )(tokens, gain8, w_gate[0], w_up[0], w_down[0], routes, route_weights, last8)
+
+
 def solution(mesh):
     in_specs = (
         P("ep", "tp"),
@@ -67,4 +381,7 @@
         P("tp"),
     )
     out_specs = P("ep", "tp")
-    return jax.shard_map(local, mesh=mesh, in_specs=in_specs, out_specs=out_specs, check_vma=False)
+    n_ep, n_tp = mesh.shape["ep"], mesh.shape["tp"]
+    square = n_tp == 4 and n_ep >= 8 and n_ep & (n_ep - 1) == 0
+    body = fused if square else local
+    return jax.shard_map(body, mesh=mesh, in_specs=in_specs, out_specs=out_specs, check_vma=False)

time: 248 us -> 116 us (0.47)
  waiting for transfers between devices: 128 us -> 0 us
  Pallas kernels: 0 us -> 107 us
  blocking collectives: 51.7 us -> 0 us
  matrix products: 33.8 us -> 0 us
  between operations: 13.6 us -> 0.01 us
  other arithmetic: 5.79 us -> 0 us
  starting transfers between devices: 4.83 us -> 0 us
    pallas_call x0 -> x1, Pallas kernels: none -> 107 us  [fused(): pl.pallas_call(functools.partial(kernel, n_ep), out_shape=jax.ShapeDtypeS...]
    reduce_scatter x1 -> x0, waiting for transfers between devices: 52.7 us -> none  [local(): lax.psum_scatter(lax.dot_general(down_w, hidden, (((0,), (1,)), ((), ()))...]
    all_gather x1 -> x0, waiting for transfers between devices: 49.4 us -> none  [local(): piece = lax.all_gather(inbox, 'tp', axis=1, tiled=True)]
    dot_general x3 -> x0, matrix products: 33.8 us -> none  [the longest x1 21 us: local(): lax.dot_general(down_w, hidden, (((0,), (1,)), ((), ())), preferred_eleme...]
    all_to_all x1 -> x0, blocking collectives: 31.3 us -> none  [local(): lax.all_to_all(outbox, 'ep', split_axis=0, concat_axis=0, tiled=True)]
    all_to_all x1 -> x0, waiting for transfers between devices: 25.9 us -> none  [local(): lax.all_to_all(sums, 'ep', split_axis=1, concat_axis=1, tiled=True)]
    psum x2 -> x0, blocking collectives: 20.3 us -> none  [the longest x1 11.4 us: local(): input_squares = lax.psum(jnp.sum(wide * wide, axis=1), 'tp')]
    scatter x1 -> x0, local copies, waits for them, and re-layouts: 5.05 us -> none  [local(): jnp.zeros((experts * capacity, share), jnp.bfloat16).at[target]]
  transfers between devices with their start and end apart: 3 -> 0, of which waited for: 3 -> 0; matrix products, arithmetic and copies ran while one was open for 0% -> 0% of each run, Pallas kernels for 0% -> 0%
where the time goes in v1:
time: 116 us; the launch traced here: 114 us
  Pallas kernels  107 us (92%)
  local copies, waits for them, and re-layouts  7.18 us (6%)
    pallas_call x1, Pallas kernels, fused(): pl.pallas_call(functools.partial(kernel, n_ep), out_shape=jax.ShapeDtypeS...  107 us
    unnamed x3, local copies, waits for them, and re-layouts  4.62 us

profile of v1, /device:TPU:0, one launch (start us, length us, event | category | flops | bytes accessed | tf_op | source)
XLA Modules:
  0.0 114.0 jit_solution(12989234594648391739)
XLA Ops:
  0.0 1.3 %broadcast_in_dim.4.gain = f32[8,512]{1,0:T(8,128)} broadcast(bf16[512]{0:T(512)(128)(2,1)} %param.9), dimensions={1} | broadcast | bytes 17408 | tf_op jit(solution)/shard_map/broadcast_in_dim | solution.py:337
  1.3 1.3 %broadcast_in_dim.5.final_gain = f32[8,512]{1,0:T(8,128)} broadcast(bf16[512]{0:T(512)(128)(2,1)} %param.15), dimensions={1} | broadcast | bytes 17408 | tf_op jit(solution)/shard_map/broadcast_in_dim | solution.py:338
  2.6 1.5 %copy.9.routes = s32[256,2]{1,0:T(8,128)} copy(s32[256,2]{0,1:T(2,128)} %param.13) | data formatting | bytes 4096 | tf_op args[5]
  4.0 1.5 %copy.10.weights = f32[256,2]{1,0:T(8,128)} copy(f32[256,2]{0,1:T(2,128)} %param.14) | data formatting | bytes 4096 | tf_op args[6]
  5.5 106.8 %routed_experts.1 = bf16[256,512]{1,0:T(8,128)(2,1)} custom-call(bf16[256,512]{1,0:T(8,128)(2,1)} %tokens.1, f32[8,512]{1,0:T(8,128)} %broadcast_in_dim.4.gain, bf16[2048,1536]{1,0:T(8,128)(2,1)} %bitcast.3, bf16[2048,1536]{1,0:T(8,128)(2,1)} %bitcast.4, bf16[1536,2048]{1,0:T(8,128)(2,1)} %bitcast.5, s32[256,2]{1,0:T(8,128)} %copy.9.routes, ...), custom_call_target="tpu_custom_call" | custom-call | tf_op jit(solution)/shard_map/routed_experts/pallas_call | solution.py:339
  112.3 1.7 %copy.12 = bf16[256,512]{1,0:T(8,128)(2,1)} copy(bf16[256,512]{1,0:T(8,128)(2,1)} %routed_experts.1) | data formatting | bytes 524288

commit v2 on v1

--- a/solution.py
+++ b/solution.py
@@ -69,13 +69,13 @@
 
 
 def kernel(
-    n_ep, tokens, gain, wg_hbm, wu_hbm, wd_hbm, routes, weights, final_gain, out,
+    n_ep, tokens, gains, wg_hbm, wu_hbm, wd_hbm, routes, weights, last, out,
     wg, wu, wd, pick, outbox, xbuf, gbuf, normed, hidden, pbuf, r1, s1, r2, fin, ret, stat,
     w_sem, z_send, z_recv, ag_send, ag_recv, g_send, g_recv, r1_send, r1_recv,
     r2_send, r2_recv, ret_send, ret_recv, st_send, st_recv,
 ):
     rows, share = tokens.shape
-    topk = routes.shape[1]
+    topk = routes.shape[0]
     cap = outbox.shape[1]
     width = 4 * share
     pairs = n_ep // 2
@@ -103,8 +103,13 @@
     for peer in tp_peers:
         pl.semaphore_signal(barrier, inc=1, device_id={"tp": peer}, device_id_type=pl.DeviceIdType.MESH)
 
+    same = lax.broadcasted_iota(jnp.int32, (rows, rows), 0) == lax.broadcasted_iota(jnp.int32, (rows, rows), 1)
+
+    def upright(line):
+        return jnp.sum(jnp.where(same, line, 0.0), axis=1, keepdims=True)
+
     lane = lax.broadcasted_iota(jnp.int32, (rows, 128), 1)
-    named = [routes[:, k : k + 1] for k in range(topk)]
+    named = [upright(routes[k : k + 1, :].astype(F32)).astype(jnp.int32) for k in range(topk)]
     hot = sum((lane == named[k]).astype(F32) for k in range(topk)).astype(BF16)
     earlier = (
         lax.broadcasted_iota(jnp.int32, (rows, rows), 1) < lax.broadcasted_iota(jnp.int32, (rows, rows), 0)
@@ -115,17 +120,20 @@
         slot = jnp.sum(jnp.where(lane == named[k], before, 0.0), axis=1, keepdims=True)
         target = named[k] * cap + slot.astype(jnp.int32)
         pick[k] = (column == target).astype(F32).astype(BF16)
-    for e in range(n_ep):
-        both = sum(pick[k, :, e * cap : (e + 1) * cap].astype(F32) for k in range(topk)).astype(BF16)
-        outbox[e] = lax.dot_general(
+    gbuf[q] = jnp.broadcast_to(gains[0:1, :].astype(F32), (8, share))
+
+    def chosen(k):
+        cols = pl.ds(pl.multiple_of(flip(k) * cap, cap), cap)
+        both = sum(pick[i, :, cols].astype(F32) for i in range(topk)).astype(BF16)
+        return lax.dot_general(
             both, tokens[...], (((0,), (0,)), ((), ())), preferred_element_type=F32
         ).astype(BF16)
-    gbuf[q] = gain[...]
-    xbuf[me, q] = outbox[me]
+
+    xbuf[me, q] = chosen(0)
     pl.semaphore_wait(barrier, n_ep - 1 + 3)
 
     def gain_copy(i):
-        return remote(gain, gbuf.at[q], g_send.at[i], g_recv.at[i], {"tp": tp_peers[i]})
+        return remote(gbuf.at[q], gbuf.at[q], g_send.at[i], g_recv.at[i], {"tp": tp_peers[i]})
 
     def out_copy(k):
         c = flip(k)
@@ -157,12 +165,7 @@
     def gather_first(s):
         for p in range(2):
             k = 2 * s + p
-            if p == 0:
-                @pl.when(s > 0)
-                def _():
-                    out_copy(k).wait_recv()
-            else:
-                out_copy(k).wait_recv()
+            out_copy(k).wait_recv()
             spread(k, p).start()
             spread(k, 1 - p).start()
 
@@ -172,7 +175,7 @@
             spread(k, p).wait_recv()
             spread(k, 2, 1 - p).start()
 
-    def compute(s):
+    def gate_up(s):
         for p in range(2):
             k = 2 * s + p
             c = flip(k)
@@ -202,6 +205,7 @@
             up = jnp.dot(normed[...], wu[:, cols], preferred_element_type=F32)
             hidden[:, cols] = (gate / (1.0 + jnp.exp(-gate)) * up).astype(BF16)
 
+    def down(s):
         @pl.when(s == 0)
         def _():
             loads[2].wait()
@@ -245,14 +249,19 @@
                 fin[c] = total
                 back(k).start()
 
-    for k in range(1, n_ep):
-        out_copy(k).start()
     for i in range(3):
         gain_copy(i).start()
-    gather_first(0)
+    spread(0, 0).start()
+    spread(0, 1).start()
+    for k in range(1, n_ep):
+        outbox[flip(k)] = chosen(k)
+        out_copy(k).start()
+        if k == 3:
+            out_copy(1).wait_recv()
+            spread(1, 1).start()
+            spread(1, 0).start()
+    gather_second(0)
     gather_first(1)
-    gather_second(0)
-    gather_first(2)
     for i in range(3):
         gain_copy(i).wait_recv()
 
@@ -260,15 +269,19 @@
     def _(s):
         @pl.when(s < pairs)
         def _():
-            compute(s)
+            gate_up(s)
 
         @pl.when(s + 1 < pairs)
         def _():
             gather_second(s + 1)
 
-        @pl.when(s + 3 < pairs)
-        def _():
-            gather_first(s + 3)
+        @pl.when(s + 2 < pairs)
+        def _():
+            gather_first(s + 2)
+
+        @pl.when(s < pairs)
+        def _():
+            down(s)
 
         @pl.when((s >= 1) & (s < pairs + 1))
         def _():
@@ -285,9 +298,8 @@
         rowsof = jnp.dot(
             pick[k], ret[...].reshape(n_ep * cap, share), preferred_element_type=F32
         )
-        combined = combined + rowsof * weights[:, k : k + 1]
+        combined = combined + rowsof * upright(weights[k : k + 1, :])
     squares = jnp.sum(combined * combined, axis=1, keepdims=True)
-    same = lax.broadcasted_iota(jnp.int32, (rows, rows), 0) == lax.broadcasted_iota(jnp.int32, (rows, rows), 1)
     line = jnp.sum(jnp.where(same, squares, 0.0), axis=0, keepdims=True)
     stat[0] = jnp.broadcast_to(line, (8, rows))
 
@@ -299,8 +311,8 @@
     for i in range(3):
         stat_copy(i).wait_recv()
     total = stat[0, 0:1] + stat[1, 0:1] + stat[2, 0:1] + stat[3, 0:1]
-    scale = lax.rsqrt(jnp.sum(jnp.where(same, total, 0.0), axis=1, keepdims=True) / width + EPS)
-    out[...] = (combined * scale * final_gain[0:1, :]).astype(BF16)
+    scale = lax.rsqrt(upright(total) / width + EPS)
+    out[...] = (combined * scale * last[0:1, :].astype(F32)).astype(BF16)
 
     for i in range(3):
         gain_copy(i).wait_send()
@@ -334,8 +346,6 @@
     dma = pltpu.SemaphoreType.DMA
     vmem = pl.BlockSpec(memory_space=pltpu.VMEM)
     hbm = pl.BlockSpec(memory_space=pl.ANY)
-    gain8 = jnp.broadcast_to(norm_gain.astype(F32)[None, :], (8, share))
-    last8 = jnp.broadcast_to(final_gain.astype(F32)[None, :], (8, share))
     return pl.pallas_call(
         functools.partial(kernel, n_ep),
         out_shape=jax.ShapeDtypeStruct((rows, share), BF16),
@@ -366,7 +376,10 @@
             collective_id=0, has_side_effects=True, vmem_limit_bytes=VMEM_LIMIT
         ),
         name="routed_experts",
-    )(tokens, gain8, w_gate[0], w_up[0], w_down[0], routes, route_weights, last8)
+    )(
+        tokens, norm_gain[None, :], w_gate[0], w_up[0], w_down[0], routes.T, route_weights.T,
+        final_gain[None, :],
+    )
 
 
 def solution(mesh):

time: 116 us -> 103 us (0.89)
  Pallas kernels: 107 us -> 97.7 us
  local copies, waits for them, and re-layouts: 7.18 us -> 4.18 us
    pallas_call x1, Pallas kernels: 107 us -> 97.7 us  [fused(): pl.pallas_call(functools.partial(kernel, n_ep), out_shape=jax.ShapeDtypeS...]
    unnamed x3 -> x1, local copies, waits for them, and re-layouts: 4.62 us -> 1.67 us
where the time goes in v2:
time: 103 us; the launch traced here: 102 us
  Pallas kernels  97.7 us (95%)
  local copies, waits for them, and re-layouts  4.18 us (4%)
    pallas_call x1, Pallas kernels, fused(): pl.pallas_call(functools.partial(kernel, n_ep), out_shape=jax.ShapeDtypeS...  97.7 us

profile of v2, /device:TPU:0, one launch (start us, length us, event | category | flops | bytes accessed | tf_op | source)
XLA Modules:
  0.0 101.9 jit_solution(16459163106333355727)
XLA Ops:
  0.0 1.3 %broadcast_in_dim.6.gains = bf16[1,512]{1,0:T(2,128)(2,1)} reshape(bf16[512]{0:T(512)(128)(2,1)} %param.9) | data formatting | bytes 2048 | tf_op jit(solution)/shard_map/broadcast_in_dim | solution.py:380
  1.3 1.3 %broadcast_in_dim.7.last = bf16[1,512]{1,0:T(2,128)(2,1)} reshape(bf16[512]{0:T(512)(128)(2,1)} %param.15) | data formatting | bytes 2048 | tf_op jit(solution)/shard_map/broadcast_in_dim | solution.py:381
  2.5 97.7 %routed_experts.1 = bf16[256,512]{1,0:T(8,128)(2,1)} custom-call(bf16[256,512]{1,0:T(8,128)(2,1)} %tokens.1, bf16[1,512]{1,0:T(2,128)(2,1)} %broadcast_in_dim.6.gains, bf16[2048,1536]{1,0:T(8,128)(2,1)} %bitcast.5, bf16[2048,1536]{1,0:T(8,128)(2,1)} %bitcast.6, bf16[1536,2048]{1,0:T(8,128)(2,1)} %bitcast.7, s32[2,256]{1,0:T(2,128)} %bitcast.8, ...), custom_call_target="tpu_custom_call" | custom-call | tf_op jit(solution)/shard_map/routed_experts/pallas_call | solution.py:349
  100.3 1.7 %copy.10 = bf16[256,512]{1,0:T(8,128)(2,1)} copy(bf16[256,512]{1,0:T(8,128)(2,1)} %routed_experts.1) | data formatting | bytes 524288
